TPU v7x, 32 devices: a whole 2x2x4 slice. The times are simulated.
32 devices in a mesh: rep: 1, fs: 8 (over z, y), tp: 4 (over x, core).
Axes of the slice: x: 2, y: 2, z: 4, core: 2. Of those that a mesh axis runs over, the one named last changes fastest.
Arguments:
- tokens: bfloat16 [4096, 2048], P(('rep', 'fs')), may hold values from -6 to 6
- gate_outer: bfloat16 [2048, 1024], P('fs', 'tp'), may hold values from -0.125 to 0.125
- gate_inner: bfloat16 [2048, 1024], P('fs', 'tp'), may hold values from -0.125 to 0.125
- conv_input: bfloat16 [2048, 1024], P('fs', 'tp'), may hold values from -0.125 to 0.125
- mixer_output: bfloat16 [2048, 1024], P('fs', 'tp'), may hold values from -0.1875 to 0.1875
- conv_taps: float32 [3, 1024], P(None, 'tp'), may hold values from -3 to 3
- mixer_gain: float32 [2048], replicated, may hold values from 0.1 to 1.9
- mixer_shift: float32 [2048], replicated, may hold values from -3 to 3
- up_weight: bfloat16 [2048, 8192], P('fs', 'tp'), may hold values from -0.125 to 0.125
- down_weight: bfloat16 [2048, 8192], P('fs', 'tp'), may hold values from -0.0625 to 0.0625
- channel_gain: float32 [2048], replicated, may hold values from 0.1 to 1.9
- channel_shift: float32 [2048], replicated, may hold values from -3 to 3
Outputs:
- mixed: bfloat16 [4096, 2048], P(('rep', 'fs'))
All inputs are finite; a program needn't handle non-finite values.
Results may differ from a plain program's by a relative error of at most 0.014.
Values may be sent and summed in bfloat16 or wider, within the bound.
A program may use at most 64 MiB of HBM per device.

v0:
```python
import functools

import jax
import jax.numpy as jnp
from jax import lax
from jax.experimental import pallas as pl
from jax.experimental.pallas import tpu as pltpu
from jax.sharding import PartitionSpec as P

residual_scale = 8.0**0.25
norm_epsilon = 1e-05
MESH = pl.DeviceIdType.MESH
f32 = jnp.float32
bf16 = jnp.bfloat16
NT = (((1,), (1,)), ((), ()))


def layer_norm(values, gain, shift):
    row_mean = jnp.mean(values, -1, keepdims=True)
    centered = values - row_mean
    variance = jnp.mean(centered * centered, -1, keepdims=True)
    return centered * lax.rsqrt(variance + norm_epsilon) * gain + shift


def kernel(
    n_fs,
    n_tp,
    via,
    tokens,
    w_go,
    w_gi,
    w_ci,
    w_mo,
    taps,
    m_gain,
    m_shift,
    w_up,
    w_dn,
    c_gain,
    c_shift,
    out,
    mix_g,
    up_g,
    dn_g,
    outer,
    zpad,
    conv,
    part,
    part2,
    first,
    hidden,
    result,
    recv1,
    recv2,
    local_sem,
    gs_send,
    gs_recv,
    ts_send,
    ts_recv,
    ms_send,
    ms_recv,
    ps_send,
    ps_recv,
):
    seq, width = tokens.shape
    rows = w_up.shape[0]
    units = w_up.shape[1]
    bits = n_tp.bit_length() - 1
    nk = n_fs // 2
    f = lax.axis_index("fs")
    t = lax.axis_index("tp")
    k = f // 2
    p = f % 2
    partner = f + 1 - 2 * p
    e = k % 2
    mate = f + 2 - 4 * e
    half = units // 2
    mine_off = e * seq
    mate_off = (1 - e) * seq
    has_right = k < nk - 1
    has_left = k > 0
    has_right2 = k < nk - 2
    has_left2 = k > 1

    def flip(bit):
        return t + bit - 2 * bit * ((t // bit) % 2)

    own = pl.ds(pl.multiple_of(f * rows, rows), rows)
    copies = []
    for j, ref in enumerate((w_go, w_gi, w_ci, w_mo)):
        copies.append(pltpu.make_async_copy(ref, mix_g.at[j, own], local_sem.at[j]))
    keep_cols = pl.ds(pl.multiple_of(e * half, half), half)
    away_cols = pl.ds(pl.multiple_of((1 - e) * half, half), half)
    for j, (w, g) in enumerate(((w_up, up_g), (w_dn, dn_g))):
        copies.append(pltpu.make_async_copy(w.at[:, keep_cols], g.at[own], local_sem.at[4 + j]))
    for c in copies:
        c.start()

    barrier = pltpu.get_barrier_semaphore()
    pl.semaphore_signal(barrier, inc=1, device_id={"fs": partner}, device_id_type=MESH)

    @pl.when(has_right)
    def _():
        pl.semaphore_signal(barrier, inc=1, device_id={"fs": f + 2}, device_id_type=MESH)

    @pl.when(has_left)
    def _():
        pl.semaphore_signal(barrier, inc=1, device_id={"fs": f - 2}, device_id_type=MESH)

    @pl.when(has_right2)
    def _():
        pl.semaphore_signal(barrier, inc=1, device_id={"fs": f + 4}, device_id_type=MESH)

    @pl.when(has_left2)
    def _():
        pl.semaphore_signal(barrier, inc=1, device_id={"fs": f - 4}, device_id_type=MESH)

    for b in range(bits):
        pl.semaphore_signal(barrier, inc=1, device_id={"tp": flip(1 << b)}, device_id_type=MESH)
    neighbours = (k + nk - 1) // nk + (2 * nk - 2 - k) // nk
    neighbours += (k + nk - 2) // nk + (2 * nk - 3 - k) // nk
    pl.semaphore_wait(barrier, 1 + bits + neighbours)

    for c in copies:
        c.wait()

    spans = ((0, rows - via), (rows - via, via))

    def piece(a, s, q):
        lo, n = spans[q]
        at = pl.ds(pl.multiple_of(s * rows + lo, 16), n)
        return mix_g.at[:, at]

    def copy(a, s, q, way):
        target = (partner, f + 2, f - 2)[way]
        ref = piece(a, s, q)
        return pltpu.make_async_remote_copy(
            src_ref=ref,
            dst_ref=ref,
            send_sem=gs_send.at[a, s, q, way],
            recv_sem=gs_recv.at[a, s, q],
            device_id={"fs": target},
            device_id_type=MESH,
        )

    def send(a, s, q, way):
        if way == 0:
            copy(a, s, q, 0).start()
        else:

            @pl.when(has_right if way == 1 else has_left)
            def _():
                copy(a, s, q, way).start()

    def arrive(a, s, q):
        copy(a, s, q, 0).wait_recv()

    def begin(a):
        for q in (0, 1):
            for way in (0, 1, 2):
                send(a, f, q, way)

    def after_pair(a):
        arrive(a, partner, 0)
        send(a, partner, 0, 1)
        send(a, partner, 0, 2)

    def step(a, d):
        for way, s, ok in ((1, f - 2 * d, k - d >= 0), (2, f + 2 * d, k + d < nk)):

            @pl.when(ok)
            def _(way=way, s=s):
                other = s + 1 - 2 * p
                for q in (1, 0):
                    arrive(a, s, q)
                    if q == 1:
                        send(a, s, q, 0)
                    send(a, s, q, way)
                arrive(a, other, 0)
                send(a, other, 0, way)

    def finish(a):
        arrive(a, partner, 1)
        for d in range(1, nk):
            for s, ok in ((f - 2 * d, k - d >= 0), (f + 2 * d, k + d < nk)):

                @pl.when(ok)
                def _(s=s):
                    arrive(a, s + 1 - 2 * p, 1)

    def drain(a):
        for q in (0, 1):
            copy(a, f, q, 0).wait_send()
            for way, has in ((1, has_right), (2, has_left)):

                @pl.when(has)
                def _(q=q, way=way):
                    copy(a, f, q, way).wait_send()
                    if q == 0:
                        copy(a, partner, q, way).wait_send()

        for d in range(1, nk):
            for way, s, ok in ((1, f - 2 * d, k - d >= 0), (2, f + 2 * d, k + d < nk)):

                @pl.when(ok)
                def _(way=way, s=s):
                    copy(a, s, 1, 0).wait_send()

                    @pl.when(has_right if way == 1 else has_left)
                    def _():
                        copy(a, s, 0, way).wait_send()
                        copy(a, s, 1, way).wait_send()
                        copy(a, s + 1 - 2 * p, 0, way).wait_send()

    def half_copy(a, s, way):
        w, g = ((w_up, up_g), (w_dn, dn_g))[a]
        dst = g.at[pl.ds(pl.multiple_of(s * rows, rows), rows)]
        src = w.at[:, away_cols] if way > 2 else dst
        return pltpu.make_async_remote_copy(
            src_ref=src,
            dst_ref=dst,
            send_sem=ms_send.at[a, s, way],
            recv_sem=ms_recv.at[a, s],
            device_id={"fs": (partner, f + 4, f - 4, f + 2, f - 2)[way]},
            device_id_type=MESH,
        )

    exists = (None, has_right2, has_left2, has_right, has_left)

    def half_each(a, s, ways, act):
        for way in ways:
            if way == 0:
                act(half_copy(a, s, way))
            else:

                @pl.when(exists[way])
                def _(way=way):
                    act(half_copy(a, s, way))

    def half_begin(a):
        half_each(a, f, (3, 4, 1, 2, 0), lambda c: c.start())

    def half_sides(d):
        return ((1, f - 2 * d, k - d >= 0), (2, f + 2 * d, k + d < nk))

    def half_step(a, d):
        for way, s, ok in half_sides(d):

            @pl.when(ok)
            def _(way=way, s=s):
                half_copy(a, s, 0).wait_recv()
                half_each(a, s, (way, 0), lambda c: c.start())

    def half_finish(a):
        half_copy(a, partner, 0).wait_recv()
        for d in range(1, nk):
            for way, s, ok in half_sides(d):

                @pl.when(ok)
                def _(s=s):
                    half_copy(a, s + 1 - 2 * p, 0).wait_recv()

    def half_drain(a):
        half_each(a, f, (0, 1, 2, 3, 4), lambda c: c.wait_send())
        for d in range(1, nk):
            for way, s, ok in half_sides(d):

                @pl.when(ok)
                def _(way=way, s=s):
                    half_each(a, s, (way, 0), lambda c: c.wait_send())

    starts = [0]
    for b in range(bits):
        starts.append(starts[-1] + ((t // (1 << b)) % 2) * (seq >> (b + 1)))

    def block_rows(start, b, off=0):
        return pl.ds(pl.multiple_of(off + start, seq >> b), seq >> b)

    def tp_copy(kind, src, dst, b):
        return pltpu.make_async_remote_copy(
            src_ref=src,
            dst_ref=dst,
            send_sem=ts_send.at[kind, b],
            recv_sem=ts_recv.at[kind, b],
            device_id={"tp": flip(1 << b)},
            device_id_type=MESH,
        )

    def reduce_copy(kind, source, landing, b, off=0, land=0):
        n = seq >> (b + 1)
        away = starts[b] + (1 - (t // (1 << b)) % 2) * n
        base = land + seq - (seq >> b)
        return tp_copy(
            kind, source.at[block_rows(away, b + 1, off)], landing.at[pl.ds(base, n)], b
        )

    def add_rows(source, start, landing, base, n):
        tile = min(n, 16)

        @pl.loop(0, n // tile)
        def _(i):
            mine = pl.ds(pl.multiple_of(start + i * tile, tile), tile)
            theirs = pl.ds(pl.multiple_of(base + i * tile, tile), tile)
            source[mine] = (source[mine].astype(f32) + landing[theirs].astype(f32)).astype(bf16)

    def reduce_add(source, landing, b, off=0, land=0):
        add_rows(source, off + starts[b + 1], landing, land + seq - (seq >> b), seq >> (b + 1))

    def gather_copy(kind, buf, b, off=0):
        ref = buf.at[block_rows(starts[b + 1], b + 1, off)]
        return tp_copy(kind, ref, ref, b)

    def pair_copy(i, src, dst, to_mate):
        return pltpu.make_async_remote_copy(
            src_ref=src,
            dst_ref=dst,
            send_sem=ps_send.at[i],
            recv_sem=ps_recv.at[i],
            device_id={"fs": mate} if to_mate else {"tp": flip(1)},
            device_id_type=MESH,
        )

    def norm_own(residual, source, landing, gain, shift, dest, off_r, off_s, land, off_d):
        n = seq >> bits
        base = land + seq - (seq >> (bits - 1))
        tile = min(n, 16)

        @pl.loop(0, n // tile)
        def _(i):
            at = starts[bits] + i * tile

            def rows_at(off):
                return pl.ds(pl.multiple_of(off + at, tile), tile)

            theirs = pl.ds(pl.multiple_of(base + i * tile, tile), tile)
            total = source[rows_at(off_s)].astype(f32) + landing[theirs].astype(f32)
            dest[rows_at(off_d)] = layer_norm(
                residual_scale * residual[rows_at(off_r)].astype(f32) + total,
                gain[...],
                shift[...],
            ).astype(bf16)

    begin(0)
    after_pair(0)
    for d in range(1, nk):
        step(0, d)
    half_begin(0)
    finish(0)

    pad = zpad.shape[0] - seq
    zpad[0:pad] = jnp.zeros((pad, zpad.shape[1]), f32)
    tile = seq // 2

    @pl.loop(0, 2)
    def _(i):
        at = pl.ds(pl.multiple_of(i * tile, tile), tile)
        x = tokens[at]
        outer[at] = jnp.dot(x, mix_g[0], preferred_element_type=f32)
        inner = jnp.dot(x, mix_g[1], preferred_element_type=f32)
        values = jnp.dot(x, mix_g[2], preferred_element_type=f32)
        zpad[pl.ds(pl.multiple_of(i * tile + pad, 8), tile)] = inner * values

    n_taps = taps.shape[0]
    acc = jnp.zeros((seq, zpad.shape[1]), f32)
    for j in range(n_taps):
        lo = pad - (n_taps - 1) + j
        acc = acc + taps[j : j + 1] * zpad[lo : lo + seq]
    conv[...] = (outer[...] * acc).astype(bf16)
    wide = min(256, width)

    @pl.loop(0, width // wide)
    def _(i):
        at = pl.ds(pl.multiple_of(i * wide, wide), wide)
        part[:, at] = lax.dot_general(
            conv[...], mix_g[3, at], NT, preferred_element_type=f32
        ).astype(bf16)

    stages = []
    for b in range(bits):
        c = reduce_copy(0, part, recv1, b)
        stages.append(c.start)
        if b < bits - 1:
            stages.append(lambda c=c, b=b: (c.wait_recv(), reduce_add(part, recv1, b)))
        else:
            stages.append(
                lambda c=c: (
                    c.wait_recv(),
                    norm_own(tokens, part, recv1, m_gain, m_shift, first, 0, 0, 0, mine_off),
                )
            )
    n0 = seq // 2
    for b in reversed(range(1, bits)):
        c = gather_copy(1, first, b, mine_off)
        stages.append(c.start)
        stages.append(c.wait_recv)
    held = first.at[block_rows(starts[1], 1, mine_off)]
    to_mate = pair_copy(0, held, held, True)
    stages.append(to_mate.start)
    stages.append(to_mate.wait_recv)
    across = []
    for q in (0, 1):
        ref = first.at[block_rows(starts[1], 1, q * seq)]
        across.append(pair_copy(1 + q, ref, ref, False))
    stages.append(lambda: [c.start() for c in across])
    stages.append(lambda: [c.wait_recv() for c in across])
    groups = [stages[:1]]
    for i in range(1, len(stages) - 1, 2):
        groups.append(stages[i : i + 2])
    groups.append(stages[-1:])

    def run(group):
        for g in group:
            g()

    run(groups.pop(0))
    for d in range(1, nk):
        if groups:
            run(groups.pop(0))
        half_step(0, d)
    half_begin(1)
    half_step(1, 1)
    while groups:
        run(groups.pop(0))
    half_finish(0)

    wide_u = min(256, half)

    @pl.loop(0, half // wide_u)
    def _(i):
        at = pl.ds(pl.multiple_of(i * wide_u, wide_u), wide_u)
        u = jnp.maximum(jnp.dot(first[...], up_g[:, at], preferred_element_type=f32), 0.0)
        hidden[:, at] = (u * u).astype(bf16)

    for d in range(2, nk):
        half_step(1, d)
    half_finish(1)

    @pl.loop(0, width // wide)
    def _(i):
        at = pl.ds(pl.multiple_of(i * wide, wide), wide)
        part2[:, at] = lax.dot_general(
            hidden[...], dn_g[at], NT, preferred_element_type=f32
        ).astype(bf16)

    over = []
    for q in (0, 1):
        away = (1 - t % 2) * n0
        over.append(
            pair_copy(
                3 + q, part2.at[block_rows(away, 1, q * seq)], recv2.at[pl.ds(q * n0, n0)], False
            )
        )
    for c in over:
        c.start()
    for c in over:
        c.wait_recv()
    add_rows(part2, mate_off + starts[1], recv2, (1 - e) * n0, n0)
    swap = pair_copy(
        5, part2.at[block_rows(starts[1], 1, mate_off)], recv2.at[pl.ds(seq, n0)], True
    )
    swap.start()
    add_rows(part2, mine_off + starts[1], recv2, e * n0, n0)
    swap.wait_recv()
    add_rows(part2, mine_off + starts[1], recv2, seq, n0)
    for b in range(1, bits):
        c = reduce_copy(2, part2, recv2, b, mine_off, seq)
        c.start()
        c.wait_recv()
        if b < bits - 1:
            reduce_add(part2, recv2, b, mine_off, seq)
    norm_own(first, part2, recv2, c_gain, c_shift, result, mine_off, mine_off, seq, 0)
    for b in reversed(range(bits)):
        c = gather_copy(3, result, b)
        c.start()
        c.wait_recv()
    done = pltpu.make_async_copy(result, out, local_sem.at[6])
    done.start()

    drain(0)
    half_drain(0)
    half_drain(1)
    for b in range(bits):
        reduce_copy(0, part, recv1, b).wait_send()
        gather_copy(3, result, b).wait_send()
        if b > 0:
            gather_copy(1, first, b, mine_off).wait_send()
            reduce_copy(2, part2, recv2, b, mine_off, seq).wait_send()
    for c in [to_mate, swap] + across + over:
        c.wait_send()
    done.wait()


def local(
    tokens,
    gate_outer,
    gate_inner,
    conv_input,
    mixer_output,
    conv_taps,
    mixer_gain,
    mixer_shift,
    up_weight,
    down_weight,
    channel_gain,
    channel_shift,
):
    seq, width = tokens.shape
    rows, units = up_weight.shape
    chans = gate_outer.shape[1]
    n_fs = lax.axis_size("fs")
    n_tp = lax.axis_size("tp")
    bits = n_tp.bit_length() - 1
    via = max(16, rows * 13 // 16 // 16 * 16)
    vmem = pl.BlockSpec(memory_space=pltpu.VMEM)
    return pl.pallas_call(
        functools.partial(kernel, n_fs, n_tp, via),
        out_shape=jax.ShapeDtypeStruct((seq, width), bf16),
        in_specs=[vmem] * 12,
        out_specs=pl.BlockSpec(memory_space=pl.ANY),
        scratch_shapes=[
            pltpu.VMEM((4, width, chans), bf16),
            pltpu.VMEM((width, units // 2), bf16),
            pltpu.VMEM((width, units // 2), bf16),
            pltpu.VMEM((seq, chans), f32),
            pltpu.VMEM((seq + 8, chans), f32),
            pltpu.VMEM((seq, chans), bf16),
            pltpu.VMEM((seq, width), bf16),
            pltpu.VMEM((2 * seq, width), bf16),
            pltpu.VMEM((2 * seq, width), bf16),
            pltpu.VMEM((2 * seq, units // 2), bf16),
            pltpu.VMEM((seq, width), bf16),
            pltpu.VMEM((seq, width), bf16),
            pltpu.VMEM((2 * seq, width), bf16),
            pltpu.SemaphoreType.DMA((7,)),
            pltpu.SemaphoreType.DMA((1, n_fs, 2, 3)),
            pltpu.SemaphoreType.DMA((1, n_fs, 2)),
            pltpu.SemaphoreType.DMA((4, bits)),
            pltpu.SemaphoreType.DMA((4, bits)),
            pltpu.SemaphoreType.DMA((2, n_fs, 5)),
            pltpu.SemaphoreType.DMA((2, n_fs)),
            pltpu.SemaphoreType.DMA((6,)),
            pltpu.SemaphoreType.DMA((6,)),
        ],
        compiler_params=pltpu.CompilerParams(
            collective_id=0, has_side_effects=True, vmem_limit_bytes=62 * 1024 * 1024
        ),
    )(
        tokens,
        gate_outer,
        gate_inner,
        conv_input,
        mixer_output,
        conv_taps,
        mixer_gain.reshape(1, width),
        mixer_shift.reshape(1, width),
        up_weight,
        down_weight,
        channel_gain.reshape(1, width),
        channel_shift.reshape(1, width),
    )


def solution(mesh):
    in_specs = (
        P(("rep", "fs"), None),
        P("fs", "tp"),
        P("fs", "tp"),
        P("fs", "tp"),
        P("fs", "tp"),
        P(None, "tp"),
        P(),
        P(),
        P("fs", "tp"),
        P("fs", "tp"),
        P(),
        P(),
    )
    out_specs = P(("rep", "fs"), None)
    return jax.shard_map(local, mesh=mesh, in_specs=in_specs, out_specs=out_specs, check_vma=False)
```

profile of v0, /device:TPU:11, one launch (start us, length us, event | category | flops | bytes accessed | tf_op | source)
XLA Modules:
  0.0 238.7 jit_solution(3801073151124312507)
XLA Ops:
  0.0 235.5 %shard_map.118 = bf16[512,2048]{1,0:T(8,128)(2,1)} custom-call(bf16[512,2048]{1,0:T(8,128)(2,1)} %tokens.1, bf16[256,256]{1,0:T(8,128)(2,1)} %w_go.1, bf16[256,256]{1,0:T(8,128)(2,1)} %w_gi.1, bf16[256,256]{1,0:T(8,128)(2,1)} %w_ci.1, bf16[256,256]{1,0:T(8,128)(2,1)} %w_mo.1, f32[3,256]{1,0:T(4,128)} %taps.1, f32[1,2048]{1,0:T(1,128)} %bitcast.4, ...), custom_call_target="tpu_custom_call" | custom-call | tf_op jit(solution)/shard_map/pallas_call | solution.py:515
  235.5 3.2 %copy.14 = bf16[512,2048]{1,0:T(8,128)(2,1)} copy(bf16[512,2048]{1,0:T(8,128)(2,1)} %shard_map.118) | data formatting | bytes 4194304
where the time goes:
time: 241 us; the launch traced here: 239 us
  Pallas kernels  236 us (98%)
  local copies, waits for them, and re-layouts  3.16 us (1%)
    pallas_call x1, Pallas kernels, local(): pl.pallas_call(functools.partial(kernel, n_fs, n_tp, via), out_shape=jax....  236 us

commit v1 on v0

v1 whole, which is shorter than its diff:
```python
import functools

import jax
import jax.numpy as jnp
from jax import lax
from jax.experimental import pallas as pl
from jax.experimental.pallas import tpu as pltpu
from jax.sharding import PartitionSpec as P

residual_scale = 8.0**0.25
norm_epsilon = 1e-05
MESH = pl.DeviceIdType.MESH
f32 = jnp.float32
bf16 = jnp.bfloat16
NT = (((1,), (1,)), ((), ()))


def layer_norm(values, gain, shift):
    row_mean = jnp.mean(values, -1, keepdims=True)
    centered = values - row_mean
    variance = jnp.mean(centered * centered, -1, keepdims=True)
    return centered * lax.rsqrt(variance + norm_epsilon) * gain + shift


def xor(value, mask):
    bit = 1
    while bit <= mask:
        if mask & bit:
            value = value + bit - 2 * bit * ((value // bit) % 2)
        bit *= 2
    return value


def kernel(
    n_fs,
    n_tp,
    via,
    sub,
    tokens,
    w_go,
    w_gi,
    w_ci,
    w_mo,
    taps,
    m_gain,
    m_shift,
    w_up,
    w_dn,
    c_gain,
    c_shift,
    out,
    mix_g,
    up_g,
    dn_g,
    outer,
    zpad,
    conv,
    part,
    recv,
    first,
    hidden,
    part2,
    r_core,
    r_mate,
    r_x,
    result,
    local_sem,
    out_sem,
    gs_send,
    gs_recv,
    z_sends,
    y_sends,
    f_recv,
    t_send,
    t_recv,
    s1_send,
    s1_recv,
    s2_send,
    s2_recv,
    s3_send,
    s3_recv,
    o_send,
    o_recv,
):
    seq, width = tokens.shape
    rows = w_up.shape[0]
    units = w_up.shape[1]
    half = units // 2
    bits = n_tp.bit_length() - 1
    nk = n_fs // 2
    f = lax.axis_index("fs")
    t = lax.axis_index("tp")
    k = f // 2
    p = f % 2
    partner = f + 1 - 2 * p
    e = k % 2
    mate_k = k + 1 - 2 * e
    mate = 2 * mate_k + p
    core = t % 2
    hs = seq // 2
    has_right = k < nk - 1
    has_left = k > 0

    def flip(bit):
        return t + bit - 2 * bit * ((t // bit) % 2)

    def block(s):
        return pl.ds(pl.multiple_of(s * rows, rows), rows)

    own = block(f)
    copies = []
    for j, ref in enumerate((w_go, w_gi, w_ci, w_mo)):
        copies.append(pltpu.make_async_copy(ref, mix_g.at[j, own], local_sem.at[j]))
    keep_cols = pl.ds(pl.multiple_of(e * half, half), half)
    for j, (w, g) in enumerate(((w_up, up_g), (w_dn, dn_g))):
        copies.append(pltpu.make_async_copy(w.at[:, keep_cols], g.at[own], local_sem.at[4 + j]))
    for c in copies:
        c.start()

    barrier = pltpu.get_barrier_semaphore()
    pl.semaphore_signal(barrier, inc=1, device_id={"fs": partner}, device_id_type=MESH)
    for i in range(1, nk):
        pl.semaphore_signal(
            barrier, inc=1, device_id={"fs": 2 * xor(k, i) + p}, device_id_type=MESH
        )
    for b in range(bits):
        pl.semaphore_signal(barrier, inc=1, device_id={"tp": flip(1 << b)}, device_id_type=MESH)
    pl.semaphore_wait(barrier, nk + bits)

    for c in copies:
        c.wait()

    spans = ((0, rows - via), (rows - via, via))

    def piece(s, q):
        lo, n = spans[q]
        return mix_g.at[:, pl.ds(pl.multiple_of(s * rows + lo, 16), n)]

    def copy(s, q, way):
        ref = piece(s, q)
        return pltpu.make_async_remote_copy(
            src_ref=ref,
            dst_ref=ref,
            send_sem=gs_send.at[s, q, way],
            recv_sem=gs_recv.at[s, q],
            device_id={"fs": (partner, f + 2, f - 2)[way]},
            device_id_type=MESH,
        )

    def send(s, q, way):
        if way == 0:
            copy(s, q, 0).start()
        else:

            @pl.when(has_right if way == 1 else has_left)
            def _():
                copy(s, q, way).start()

    def arrive(s, q):
        copy(s, q, 0).wait_recv()

    def sides(d):
        return ((1, f - 2 * d, k - d >= 0), (2, f + 2 * d, k + d < nk))

    def begin():
        for q in (0, 1):
            for way in (0, 1, 2):
                send(f, q, way)

    def after_pair():
        arrive(partner, 0)
        send(partner, 0, 1)
        send(partner, 0, 2)

    def step(d):
        for way, s, ok in sides(d):

            @pl.when(ok)
            def _(way=way, s=s):
                other = s + 1 - 2 * p
                for q in (1, 0):
                    arrive(s, q)
                    if q == 1:
                        send(s, q, 0)
                    send(s, q, way)
                arrive(other, 0)
                send(other, 0, way)

    def finish():
        arrive(partner, 1)
        for d in range(1, nk):
            for way, s, ok in sides(d):

                @pl.when(ok)
                def _(s=s):
                    arrive(s + 1 - 2 * p, 1)

    def drain():
        for q in (0, 1):
            copy(f, q, 0).wait_send()
            for way, has in ((1, has_right), (2, has_left)):

                @pl.when(has)
                def _(q=q, way=way):
                    copy(f, q, way).wait_send()
                    if q == 0:
                        copy(partner, q, way).wait_send()

        for d in range(1, nk):
            for way, s, ok in sides(d):

                @pl.when(ok)
                def _(way=way, s=s):
                    copy(s, 1, 0).wait_send()

                    @pl.when(has_right if way == 1 else has_left)
                    def _():
                        copy(s, 0, way).wait_send()
                        copy(s, 1, way).wait_send()
                        copy(s + 1 - 2 * p, 0, way).wait_send()

    pairs = ((w_up, up_g), (w_dn, dn_g))

    def z_copy(a, to_k):
        w, g = pairs[a]
        cols = pl.ds(pl.multiple_of((to_k % 2) * half, half), half)
        return pltpu.make_async_remote_copy(
            src_ref=w.at[:, cols],
            dst_ref=g.at[own],
            send_sem=z_sends.at[a, to_k],
            recv_sem=f_recv.at[a, f],
            device_id={"fs": 2 * to_k + p},
            device_id_type=MESH,
        )

    def y_copy(a, of_k):
        ref = pairs[a][1].at[block(2 * of_k + p)]
        return pltpu.make_async_remote_copy(
            src_ref=ref,
            dst_ref=ref,
            send_sem=y_sends.at[a, of_k],
            recv_sem=f_recv.at[a, 2 * of_k + p],
            device_id={"fs": partner},
            device_id_type=MESH,
        )

    def f_wait(a, s):
        ref = pairs[a][1].at[block(s)]
        pltpu.make_async_remote_copy(
            src_ref=ref,
            dst_ref=ref,
            send_sem=y_sends.at[a, 0],
            recv_sem=f_recv.at[a, s],
            device_id={"fs": partner},
            device_id_type=MESH,
        ).wait_recv()

    def z_right(a, d):
        @pl.when(k == d)
        def _():
            for kk in range(d + 1, nk):
                z_copy(a, kk).start()

    def z_left(a, d):
        @pl.when(k == d)
        def _():
            for kk in range(d - 1, -1, -1):
                z_copy(a, kk).start()

    def z_all(a):
        for d in range(nk):
            z_right(a, d)
            z_left(a, d)

    def relay(a, of_k):
        f_wait(a, 2 * of_k + p)
        y_copy(a, of_k).start()

    def f_drain(a):
        for kk in range(nk):
            y_copy(a, kk).wait_send()

            @pl.when(k != kk)
            def _(kk=kk):
                z_copy(a, kk).wait_send()

    group = k // 2
    order = [2 * group, 2 * group + 1]
    for m in range(1, nk // 2):
        low = (group // (1 << (m.bit_length() - 1))) % 2
        for j in (0, 1):
            order.append(2 * xor(group, m) + low * (1 - j) + (1 - low) * j)
    relays = [mate_k] + order[2:]

    starts = [0]
    for b in range(bits):
        starts.append(starts[-1] + ((t // (1 << b)) % 2) * (seq >> (b + 1)))

    def aways(b):
        return starts[b] + (1 - (t // (1 << b)) % 2) * (seq >> (b + 1))

    def span(start, n):
        return pl.ds(pl.multiple_of(start, n), n)

    def t_copy(i, src, dst, device):
        return pltpu.make_async_remote_copy(
            src_ref=src,
            dst_ref=dst,
            send_sem=t_send.at[i],
            recv_sem=t_recv.at[i],
            device_id=device,
            device_id_type=MESH,
        )

    def landing(b):
        return seq - (seq >> b)

    def reduce_copy(b):
        n = seq >> (b + 1)
        return t_copy(
            b, part.at[span(aways(b), n)], recv.at[pl.ds(landing(b), n)], {"tp": flip(1 << b)}
        )

    def add_recv(b, start, n):
        base = landing(b) - starts[b + 1]
        tile = min(n, 16)

        @pl.loop(0, n // tile)
        def _(i):
            mine = pl.ds(pl.multiple_of(start + i * tile, tile), tile)
            theirs = pl.ds(pl.multiple_of(base + start + i * tile, tile), tile)
            part[mine] = (part[mine].astype(f32) + recv[theirs].astype(f32)).astype(bf16)

    def gather_copy(i, q, b):
        ref = first.at[q, span(starts[b + 1], seq >> (b + 1))]
        return t_copy(i + b, ref, ref, {"tp": flip(1 << b)})

    begin()
    after_pair()
    z_right(0, 0)
    z_left(0, nk - 1)
    for d in range(1, nk):
        step(d)
        z_right(0, d)
        z_left(0, nk - 1 - d)
    y_copy(0, k).start()
    finish()

    pad = zpad.shape[0] - seq
    zpad[0:pad] = jnp.zeros((pad, zpad.shape[1]), f32)
    tile = seq // 2

    @pl.loop(0, 2)
    def _(i):
        at = pl.ds(pl.multiple_of(i * tile, tile), tile)
        x = tokens[at]
        outer[at] = jnp.dot(x, mix_g[0], preferred_element_type=f32)
        inner = jnp.dot(x, mix_g[1], preferred_element_type=f32)
        values = jnp.dot(x, mix_g[2], preferred_element_type=f32)
        zpad[pl.ds(pl.multiple_of(i * tile + pad, 8), tile)] = inner * values

    n_taps = taps.shape[0]
    acc = jnp.zeros((seq, zpad.shape[1]), f32)
    for j in range(n_taps):
        lo = pad - (n_taps - 1) + j
        acc = acc + taps[j : j + 1] * zpad[lo : lo + seq]
    conv[...] = (outer[...] * acc).astype(bf16)
    wide = min(256, width)

    def mix_out(start):
        at_rows = span(start, hs)
        lhs = conv[at_rows]

        @pl.loop(0, width // wide)
        def _(i):
            at = pl.ds(pl.multiple_of(i * wide, wide), wide)
            part[at_rows, at] = lax.dot_general(
                lhs, mix_g[3, at], NT, preferred_element_type=f32
            ).astype(bf16)

    mix_out(aways(0))
    reduces = [reduce_copy(b) for b in range(bits)]
    reduces[0].start()
    mix_out(starts[1])
    relay(0, relays[0])
    for b in range(1, bits):
        n = seq >> (b + 1)
        reduces[b - 1].wait_recv()
        add_recv(b - 1, aways(b), n)
        reduces[b].start()
        add_recv(b - 1, starts[b + 1], n)
    if nk > 2:
        relay(0, relays[1])
    last = bits - 1
    reduces[last].wait_recv()
    n_own = seq >> bits
    tile_n = min(n_own, 16)

    @pl.loop(0, n_own // tile_n)
    def _(i):
        at = pl.ds(pl.multiple_of(starts[bits] + i * tile_n, tile_n), tile_n)
        theirs = pl.ds(pl.multiple_of(landing(last) + i * tile_n, tile_n), tile_n)
        total = part[at].astype(f32) + recv[theirs].astype(f32)
        first[e, at] = layer_norm(
            residual_scale * tokens[at].astype(f32) + total, m_gain[...], m_shift[...]
        ).astype(bf16)

    mine_n = first.at[e, span(starts[bits], n_own)]
    to_mate = t_copy(bits, mine_n, mine_n, {"fs": mate})
    own_g = [gather_copy(bits + 1, e, b) for b in range(bits)]
    mate_g = [gather_copy(2 * bits + 1, 1 - e, b) for b in range(bits)]
    to_mate.start()
    own_g[last].start()
    z_all(1)
    for m in relays[2:-1]:
        relay(0, m)
    for b in range(last, 0, -1):
        own_g[b].wait_recv()
        own_g[b - 1].start()
    to_mate.wait_recv()
    mate_g[last].start()
    if nk > 2:
        relay(0, relays[-1])
    y_copy(1, k).start()
    own_g[0].wait_recv()
    f_wait(0, partner)
    for m in relays:
        f_wait(0, 2 * m + 1 - p)

    wide_u = min(256, half)

    def up(q):
        @pl.loop(0, half // wide_u)
        def _(i):
            at = pl.ds(pl.multiple_of(i * wide_u, wide_u), wide_u)
            u = jnp.maximum(jnp.dot(first[q], up_g[:, at], preferred_element_type=f32), 0.0)
            hidden[q, :, at] = (u * u).astype(bf16)

    up(e)
    for b in range(last, 0, -1):
        mate_g[b].wait_recv()
        mate_g[b - 1].start()
    relay(1, relays[0])
    mate_g[0].wait_recv()
    up(1 - e)

    cw = 2 * rows // sub
    mine_h = pl.ds(pl.multiple_of(core * hs, hs), hs)
    away_h = pl.ds(pl.multiple_of((1 - core) * hs, hs), hs)
    chunks = []
    for m in order:
        if sub == 2:
            chunks.append((m, (2 * m + p) * rows))
            chunks.append((m, (2 * m + 1 - p) * rows))
        else:
            chunks.append((m, 2 * m * rows))

    def cols_of(j):
        return pl.ds(pl.multiple_of(chunks[j][1], cw), cw)

    def remote(src, dst, ssem, rsem, device):
        return pltpu.make_async_remote_copy(
            src_ref=src,
            dst_ref=dst,
            send_sem=ssem,
            recv_sem=rsem,
            device_id=device,
            device_id_type=MESH,
        )

    def s1(j):
        c = cols_of(j)
        return remote(
            part2.at[:, away_h, c],
            r_core.at[:, :, c],
            s1_send.at[j],
            s1_recv.at[j],
            {"tp": flip(1)},
        )

    def s2(j):
        c = cols_of(j)
        return remote(
            part2.at[1 - e, mine_h, c],
            r_mate.at[:, c],
            s2_send.at[j],
            s2_recv.at[j],
            {"fs": mate},
        )

    def s3(j, b):
        c = cols_of(j)
        return remote(
            part2.at[e, mine_h, c],
            r_x.at[b - 1, :, c],
            s3_send.at[b - 1, j],
            s3_recv.at[b - 1, j],
            {"tp": flip(1 << b)},
        )

    def product(j):
        c = cols_of(j)
        w = dn_g[c]

        @pl.loop(0, 2)
        def _(q):
            part2[q, :, c] = lax.dot_general(
                hidden[q], w, NT, preferred_element_type=f32
            ).astype(bf16)

        s1(j).start()

    def core_sum(j):
        c = cols_of(j)
        s1(j).wait_recv()
        part2[1 - e, mine_h, c] = (
            part2[1 - e, mine_h, c].astype(f32) + r_core[1 - e, :, c].astype(f32)
        ).astype(bf16)
        s2(j).start()

    def mate_sum(j):
        c = cols_of(j)
        s2(j).wait_recv()
        part2[e, mine_h, c] = (
            part2[e, mine_h, c].astype(f32)
            + r_core[e, :, c].astype(f32)
            + r_mate[:, c].astype(f32)
        ).astype(bf16)
        s3(j, 1).start()

    def x_sum(j, b):
        c = cols_of(j)
        s3(j, b - 1).wait()
        part2[e, mine_h, c] = (
            part2[e, mine_h, c].astype(f32) + r_x[b - 2, :, c].astype(f32)
        ).astype(bf16)
        s3(j, b).start()

    stages = [core_sum, mate_sum]
    for b in range(2, bits):
        stages.append(functools.partial(x_sum, b=b))
    n_ch = len(chunks)

    def advance(j):
        for i, stage in enumerate(stages):
            if 0 <= j - 1 - i < n_ch:
                stage(j - 1 - i)

    def arrived(j):
        m = chunks[j][0]
        if sub == 1:
            f_wait_other(m, 0)
            f_wait_other(m, 1)
        else:
            f_wait_other(m, j % 2)

    def f_wait_other(m, other):
        if other:
            f_wait(1, 2 * m + 1 - p)

    for j in range(n_ch):
        n = j // sub
        if n >= 1 and j % sub == sub - 1 and n + 1 < nk:
            relay(1, order[n + 1])
        if sub == 1 and n == 1 and nk > 2:
            pass
        arrived(j)
        product(j)
        advance(j)
    for j in range(n_ch, n_ch + len(stages)):
        advance(j)

    n_out = o_send.shape[0]
    piece_rows = hs // n_out
    tile_o = min(piece_rows, 16)

    def out_rows(i):
        return pl.ds(pl.multiple_of(core * hs + i * piece_rows, piece_rows), piece_rows)

    def out_local(i):
        return pltpu.make_async_copy(
            result.at[pl.ds(i * piece_rows, piece_rows)], out.at[out_rows(i)], out_sem.at[i]
        )

    def out_remote(i):
        return remote(
            result.at[pl.ds(i * piece_rows, piece_rows)],
            out.at[out_rows(i)],
            o_send.at[i],
            o_recv.at[i],
            {"tp": flip(1)},
        )

    for j in range(n_ch):
        s3(j, last).wait_recv()
    for i in range(n_out):

        @pl.loop(0, piece_rows // tile_o)
        def _(ii):
            lo = i * piece_rows + ii * tile_o
            here = pl.ds(pl.multiple_of(lo, tile_o), tile_o)
            at = pl.ds(pl.multiple_of(core * hs + lo, tile_o), tile_o)
            total = part2[e, at].astype(f32) + r_x[last - 1, here].astype(f32)
            result[here] = layer_norm(
                residual_scale * first[e, at].astype(f32) + total, c_gain[...], c_shift[...]
            ).astype(bf16)

        out_local(i).start()
        out_remote(i).start()

    drain()
    f_drain(0)
    f_drain(1)
    for c in reduces + [to_mate] + own_g + mate_g:
        c.wait_send()
    for j in range(n_ch):
        s1(j).wait_send()
        s2(j).wait_send()
        s3(j, last).wait_send()
    for i in range(n_out):
        out_local(i).wait()
        out_remote(i).wait()


def local(
    tokens,
    gate_outer,
    gate_inner,
    conv_input,
    mixer_output,
    conv_taps,
    mixer_gain,
    mixer_shift,
    up_weight,
    down_weight,
    channel_gain,
    channel_shift,
):
    seq, width = tokens.shape
    rows, units = up_weight.shape
    chans = gate_outer.shape[1]
    half = units // 2
    n_fs = lax.axis_size("fs")
    n_tp = lax.axis_size("tp")
    bits = n_tp.bit_length() - 1
    nk = n_fs // 2
    via = max(16, rows * 13 // 16 // 16 * 16)
    sub = 2 if rows % 128 == 0 else 1
    n_ch = nk * sub
    hs = seq // 2
    n_out = 4
    n_t = 3 * bits + 1
    vmem = pl.BlockSpec(memory_space=pltpu.VMEM)
    dma = pltpu.SemaphoreType.DMA
    return pl.pallas_call(
        functools.partial(kernel, n_fs, n_tp, via, sub),
        out_shape=jax.ShapeDtypeStruct((seq, width), bf16),
        in_specs=[vmem] * 12,
        out_specs=pl.BlockSpec(memory_space=pl.ANY),
        scratch_shapes=[
            pltpu.VMEM((4, width, chans), bf16),
            pltpu.VMEM((width, half), bf16),
            pltpu.VMEM((width, half), bf16),
            pltpu.VMEM((seq, chans), f32),
            pltpu.VMEM((seq + 8, chans), f32),
            pltpu.VMEM((seq, chans), bf16),
            pltpu.VMEM((seq, width), bf16),
            pltpu.VMEM((seq, width), bf16),
            pltpu.VMEM((2, seq, width), bf16),
            pltpu.VMEM((2, seq, half), bf16),
            pltpu.VMEM((2, seq, width), bf16),
            pltpu.VMEM((2, hs, width), bf16),
            pltpu.VMEM((hs, width), bf16),
            pltpu.VMEM((bits - 1, hs, width), bf16),
            pltpu.VMEM((hs, width), bf16),
            dma((6,)),
            dma((n_out,)),
            dma((n_fs, 2, 3)),
            dma((n_fs, 2)),
            dma((2, nk)),
            dma((2, nk)),
            dma((2, n_fs)),
            dma((n_t,)),
            dma((n_t,)),
            dma((n_ch,)),
            dma((n_ch,)),
            dma((n_ch,)),
            dma((n_ch,)),
            dma((bits - 1, n_ch)),
            dma((bits - 1, n_ch)),
            dma((n_out,)),
            dma((n_out,)),
        ],
        compiler_params=pltpu.CompilerParams(
            collective_id=0, has_side_effects=True, vmem_limit_bytes=62 * 1024 * 1024
        ),
    )(
        tokens,
        gate_outer,
        gate_inner,
        conv_input,
        mixer_output,
        conv_taps,
        mixer_gain.reshape(1, width),
        mixer_shift.reshape(1, width),
        up_weight,
        down_weight,
        channel_gain.reshape(1, width),
        channel_shift.reshape(1, width),
    )


def solution(mesh):
    in_specs = (
        P(("rep", "fs"), None),
        P("fs", "tp"),
        P("fs", "tp"),
        P("fs", "tp"),
        P("fs", "tp"),
        P(None, "tp"),
        P(),
        P(),
        P("fs", "tp"),
        P("fs", "tp"),
        P(),
        P(),
    )
    out_specs = P(("rep", "fs"), None)
    return jax.shard_map(local, mesh=mesh, in_specs=in_specs, out_specs=out_specs, check_vma=False)
```

time: 241 us -> 199 us (0.83)
  Pallas kernels: 236 us -> 195 us
    pallas_call x1, Pallas kernels: 236 us -> 195 us  [local(): pl.pallas_call(functools.partial(kernel, n_fs, n_tp, via, sub), out_shape...]
where the time goes in v1:
time: 199 us
  Pallas kernels  195 us (98%)
  local copies, waits for them, and re-layouts  3.16 us (2%)
    pallas_call x1, Pallas kernels, local(): pl.pallas_call(functools.partial(kernel, n_fs, n_tp, via, sub), out_shape...  195 us

profile of v1, /device:TPU:11, one launch (start us, length us, event | category | flops | bytes accessed | tf_op | source)
XLA Modules:
  0.0 198.7 jit_solution(12926842277746717283)
XLA Ops:
  0.0 195.5 %shard_map.118 = bf16[512,2048]{1,0:T(8,128)(2,1)} custom-call(bf16[512,2048]{1,0:T(8,128)(2,1)} %tokens.1, bf16[256,256]{1,0:T(8,128)(2,1)} %w_go.1, bf16[256,256]{1,0:T(8,128)(2,1)} %w_gi.1, bf16[256,256]{1,0:T(8,128)(2,1)} %w_ci.1, bf16[256,256]{1,0:T(8,128)(2,1)} %w_mo.1, f32[3,256]{1,0:T(4,128)} %taps.1, f32[1,2048]{1,0:T(1,128)} %bitcast.4, ...), custom_call_target="tpu_custom_call" | custom-call | tf_op jit(solution)/shard_map/pallas_call | solution.py:655
  195.5 3.2 %copy.14 = bf16[512,2048]{1,0:T(8,128)(2,1)} copy(bf16[512,2048]{1,0:T(8,128)(2,1)} %shard_map.118) | data formatting | bytes 4194304

commit v2 on v1

v2 whole, which is shorter than its diff:
```python
import functools

import jax
import jax.numpy as jnp
from jax import lax
from jax.experimental import pallas as pl
from jax.experimental.pallas import tpu as pltpu
from jax.sharding import PartitionSpec as P

residual_scale = 8.0**0.25
norm_epsilon = 1e-05
MESH = pl.DeviceIdType.MESH
f32 = jnp.float32
bf16 = jnp.bfloat16
NT = (((1,), (1,)), ((), ()))


def layer_norm(values, gain, shift):
    row_mean = jnp.mean(values, -1, keepdims=True)
    centered = values - row_mean
    variance = jnp.mean(centered * centered, -1, keepdims=True)
    return centered * lax.rsqrt(variance + norm_epsilon) * gain + shift


def xor(value, mask):
    bit = 1
    while bit <= mask:
        if mask & bit:
            value = value + bit - 2 * bit * ((value // bit) % 2)
        bit *= 2
    return value


def kernel(
    n_fs,
    n_tp,
    sub,
    n_pc,
    hops,
    tokens,
    w_go,
    w_gi,
    w_ci,
    w_mo,
    taps,
    m_gain,
    m_shift,
    w_up,
    w_dn,
    c_gain,
    c_shift,
    out,
    mix_g,
    up_g,
    dn_g,
    tok_m,
    outer,
    zpad,
    conv,
    part,
    recv,
    r_sum,
    first,
    hidden,
    part2,
    r_core,
    r_mate,
    r_x,
    result,
    local_sem,
    out_sem,
    z_sends,
    y_sends,
    f_recv,
    t_send,
    t_recv,
    s1_send,
    s1_recv,
    s2_send,
    s2_recv,
    s3_send,
    s3_recv,
    o_send,
    o_recv,
):
    seq, width = tokens.shape
    rows = w_up.shape[0]
    half = w_up.shape[1] // 2
    hc = mix_g.shape[2]
    bits = n_tp.bit_length() - 1
    nk = n_fs // 2
    f = lax.axis_index("fs")
    t = lax.axis_index("tp")
    k = f // 2
    p = f % 2
    partner = f + 1 - 2 * p
    e = k % 2
    mate_k = k + 1 - 2 * e
    mate = 2 * mate_k + p
    core = t % 2
    hs = seq // 2
    inner = jnp.logical_and(k > 0, k < nk - 1)

    def flip(bit):
        return t + bit - 2 * bit * ((t // bit) % 2)

    def span(start, n):
        return pl.ds(pl.multiple_of(start, n), n)

    def remote(src, dst, ssem, rsem, device):
        return pltpu.make_async_remote_copy(
            src_ref=src,
            dst_ref=dst,
            send_sem=ssem,
            recv_sem=rsem,
            device_id=device,
            device_id_type=MESH,
        )

    sources = (w_go, w_gi, w_ci, w_mo, w_up, w_dn)
    UP, DN = 4, 5

    def pieces(a):
        return n_pc if a >= UP else 1

    def source(a, parity, q):
        w = sources[a]
        pn = rows // pieces(a)
        at = pl.ds(q * pn, pn)
        if len(w.shape) == 3:
            return w.at[parity, at]
        n = half if a >= UP else hc
        return w.at[at, span(parity * n, n)]

    def held(a, s, q):
        pn = rows // pieces(a)
        at = span(s * rows + q * pn, pn)
        if a < UP:
            return mix_g.at[a, at]
        return (up_g if a == UP else dn_g).at[at]

    copies = []
    for a in range(6):
        for q in range(pieces(a)):
            copies.append(
                pltpu.make_async_copy(source(a, e, q), held(a, f, q), local_sem.at[a, q])
            )
    for c in copies:
        c.start()

    barrier = pltpu.get_barrier_semaphore()
    pl.semaphore_signal(barrier, inc=1, device_id={"fs": partner}, device_id_type=MESH)
    for i in range(1, nk):
        pl.semaphore_signal(
            barrier, inc=1, device_id={"fs": 2 * xor(k, i) + p}, device_id_type=MESH
        )
    for b in range(bits):
        pl.semaphore_signal(barrier, inc=1, device_id={"tp": flip(1 << b)}, device_id_type=MESH)
    pl.semaphore_wait(barrier, nk + bits)

    def z_copy(a, to_k, q):
        return remote(
            source(a, to_k % 2, q),
            held(a, f, q),
            z_sends.at[a, to_k, q],
            f_recv.at[a, f, q],
            {"fs": 2 * to_k + p},
        )

    def y_copy(a, of_k, q):
        ref = held(a, 2 * of_k + p, q)
        return remote(
            ref, ref, y_sends.at[a, of_k, q], f_recv.at[a, 2 * of_k + p, q], {"fs": partner}
        )

    def f_wait(a, s, q):
        ref = held(a, s, q)
        remote(ref, ref, y_sends.at[a, 0, q], f_recv.at[a, s, q], {"fs": partner}).wait_recv()

    def z_send(a, kk):
        for q in range(pieces(a)):
            z_copy(a, kk, q).start()

    def z_right(arrays, d, lo=1, hi=None):
        @pl.when(k == d)
        def _():
            for kk in range(d + lo, nk if hi is None else min(d + hi, nk)):
                for a in arrays:
                    z_send(a, kk)

    def z_left(arrays, d, lo=1, hi=None):
        @pl.when(k == d)
        def _():
            for kk in range(d - lo, -1 if hi is None else max(d - hi, -1), -1):
                for a in arrays:
                    z_send(a, kk)

    def z_all(arrays):
        for d in range(nk):
            z_right(arrays, d)
            z_left(arrays, d)

    def z_ends(arrays, lo, hi=None):
        z_right(arrays, 0, lo, hi)
        z_left(arrays, nk - 1, lo, hi)

    def z_mid(arrays, lo=1, hi=None):
        for d in range(1, nk - 1):
            if d < nk - 2:
                z_right(arrays, d, lo, hi)
            if d > 1:
                z_left(arrays, d, lo, hi)

    def z_outward(arrays):
        z_right(arrays, nk - 2)
        z_left(arrays, 1)

    def y_own(a):
        for q in range(pieces(a)):
            y_copy(a, k, q).start()

    def relay(a, of_k, q):
        f_wait(a, 2 * of_k + p, q)
        y_copy(a, of_k, q).start()

    def relay_all(a, of_k):
        for q in range(pieces(a)):
            relay(a, of_k, q)

    def f_drain(a):
        for kk in range(nk):
            for q in range(pieces(a)):
                y_copy(a, kk, q).wait_send()

            @pl.when(k != kk)
            def _(kk=kk):
                for q in range(pieces(a)):
                    z_copy(a, kk, q).wait_send()

    group = k // 2
    order = [2 * group, 2 * group + 1]
    for m in range(1, nk // 2):
        low = (group // (1 << (m.bit_length() - 1))) % 2
        for j in (0, 1):
            order.append(2 * xor(group, m) + low * (1 - j) + (1 - low) * j)
    later = [(of_k, q) for of_k in order[2:] for q in range(n_pc)]

    def relay_some(a, lo, hi):
        for of_k, q in later[lo:hi]:
            relay(a, of_k, q)

    def partners_wait(a):
        for of_k in order:
            for q in range(pieces(a)):
                f_wait(a, 2 * of_k + 1 - p, q)

    def at_inner(fn):
        pl.when(inner)(fn)

    def at_end(fn):
        pl.when(jnp.logical_not(inner))(fn)

    starts = [0]
    for b in range(bits):
        starts.append(starts[-1] + ((t // (1 << b)) % 2) * (seq >> (b + 1)))

    def aways(b):
        return starts[b] + (1 - (t // (1 << b)) % 2) * (seq >> (b + 1))

    n_t = [0]

    def t_copy(src, dst, device):
        i = n_t[0]
        n_t[0] += 1
        return remote(src, dst, t_send.at[i], t_recv.at[i], device)

    def landing(b):
        return seq - (seq >> b)

    class Split:
        def __init__(self, n, make):
            self.parts = [make(n // hops * h, n // hops) for h in range(hops)]

        def start(self):
            for c in self.parts:
                c.start()

        def wait_recv(self):
            for c in self.parts:
                c.wait_recv()

        def wait_send(self):
            for c in self.parts:
                c.wait_send()

    def shift(start, lo, n):
        return pl.ds(pl.multiple_of(start + lo, n), n)

    def reduce_copy(i, b):
        return Split(
            seq >> (b + 1),
            lambda lo, n: t_copy(
                part.at[i, shift(aways(b), lo, n)],
                recv.at[i, pl.ds(landing(b) + lo, n)],
                {"tp": flip(1 << b)},
            ),
        )

    def add_recv(i, b, start, n, origin=None):
        base = landing(b) - (starts[b + 1] if origin is None else origin)
        tile = min(n, 64)

        @pl.loop(0, n // tile)
        def _(j):
            mine = pl.ds(pl.multiple_of(start + j * tile, tile), tile)
            theirs = pl.ds(pl.multiple_of(base + start + j * tile, tile), tile)
            part[i, mine] = (part[i, mine].astype(f32) + recv[i, theirs].astype(f32)).astype(bf16)

    last = bits - 1
    n_own = seq >> bits
    own_rows = span(starts[bits], n_own)

    tok_z = t_copy(tokens.at[own_rows], tok_m.at[own_rows], {"fs": mate})
    tok_g = []
    for b in range(bits):
        ref = tok_m.at[span(starts[b + 1], seq >> (b + 1))]
        tok_g.append(t_copy(ref, ref, {"tp": flip(1 << b)}))
    reduces = [[reduce_copy(i, b) for b in range(bits)] for i in (0, 1)]
    sum_z = Split(
        n_own,
        lambda lo, n: t_copy(
            part.at[1, shift(starts[bits], lo, n)], r_sum.at[pl.ds(lo, n)], {"fs": mate}
        ),
    )

    def mate_piece(lo, n):
        ref = first.at[e, shift(starts[bits], lo, n)]
        return t_copy(ref, ref, {"fs": mate})

    to_mate = Split(n_own, mate_piece)
    gathers = []
    for i in (e, 1 - e):
        gathers.append([])
        for b in range(bits):


            def gather_piece(lo, n):
                ref = first.at[i, shift(starts[b + 1], lo, n)]
                return t_copy(ref, ref, {"tp": flip(1 << b)})

            gathers[-1].append(Split(seq >> (b + 1), gather_piece))
    own_g, mate_g = gathers

    ins = (0, 1, 2)
    tok_z.start()
    z_all(ins)
    z_all((3,))
    z_all((UP,))
    for c in copies:
        c.wait()
    for a in range(UP + 1):
        y_own(a)
    tok_z.wait_recv()
    tok_g[last].start()
    for of_k in [mate_k] + order[2:3]:
        for a in ins:
            relay(a, of_k, 0)
    for b in range(last, 0, -1):
        tok_g[b].wait_recv()
        tok_g[b - 1].start()
    for of_k in order[3:]:
        for a in ins:
            relay(a, of_k, 0)
    for of_k in [mate_k] + order[2:]:
        relay(3, of_k, 0)
    tok_g[0].wait_recv()
    for a in ins:
        partners_wait(a)

    @at_inner
    def _():
        relay_all(UP, mate_k)

    at_end(lambda: y_own(DN))

    pad = zpad.shape[1] - seq
    n_taps = taps.shape[0]
    tile = min(256, seq)

    def project(i, x_ref):
        zpad[i, 0:pad] = jnp.zeros((pad, hc), f32)

        @pl.loop(0, seq // tile)
        def _(j):
            at = pl.ds(pl.multiple_of(j * tile, tile), tile)
            x = x_ref[at]
            if hc % 128 == 0:
                w = jnp.concatenate([mix_g[a] for a in ins], axis=1)
                y = jnp.dot(x, w, preferred_element_type=f32)
                ys = [y[:, a * hc : (a + 1) * hc] for a in ins]
            else:
                ys = [jnp.dot(x, mix_g[a], preferred_element_type=f32) for a in ins]
            outer[i, at] = ys[0]
            zpad[i, pl.ds(pl.multiple_of(j * tile + pad, 8), tile)] = ys[1] * ys[2]

        acc = jnp.zeros((seq, hc), f32)
        for j in range(n_taps):
            lo = pad - (n_taps - 1) + j
            acc = acc + tap_rows[j : j + 1] * zpad[i, lo : lo + seq]
        conv[i] = (outer[i] * acc).astype(bf16)

    if len(taps.shape) == 3:
        tap_rows = taps[:, e, :]
    else:
        tap_rows = taps[:, span(e * hc, hc)]
    wide = min(256, width)

    def mix_out(i, start):
        at_rows = span(start, hs)
        lhs = conv[i, at_rows]

        @pl.loop(0, width // wide)
        def _(j):
            at = pl.ds(pl.multiple_of(j * wide, wide), wide)
            part[i, at_rows, at] = lax.dot_general(
                lhs, mix_g[3, at], NT, preferred_element_type=f32
            ).astype(bf16)

    def stage_up(i, b):
        n = seq >> (b + 1)
        reduces[i][b - 1].wait_recv()
        add_recv(i, b - 1, aways(b), n)
        reduces[i][b].start()
        add_recv(i, b - 1, starts[b + 1], n)

    for i, x_ref in ((1, tok_m), (0, tokens)):
        project(i, x_ref)
        if i:
            partners_wait(3)
        mix_out(i, aways(0))
        reduces[i][0].start()
        mix_out(i, starts[1])
        stage_up(i, 1)
    for b in range(2, bits):
        for i in (1, 0):
            stage_up(i, b)

    n_l = len(later)
    early = n_pc // 2

    @at_end
    def _():
        relay_all(UP, mate_k)

    at_inner(lambda: relay_some(UP, 0, n_pc))
    for h in range(hops):
        n_h = n_own // hops
        reduces[1][last].parts[h].wait_recv()
        add_recv(1, last, starts[bits] + h * n_h, n_h, starts[bits])
        sum_z.parts[h].start()
    z_mid((DN,), 1, 2)
    at_end(lambda: relay_some(UP, 0, n_pc))
    relay_some(UP, n_pc, n_l)
    at_inner(lambda: y_own(DN))
    reduces[0][last].wait_recv()
    sum_z.wait_recv()
    tile_n = min(n_own, 64)

    @pl.loop(0, n_own // tile_n)
    def _(i):
        at = pl.ds(pl.multiple_of(starts[bits] + i * tile_n, tile_n), tile_n)
        here = pl.ds(pl.multiple_of(i * tile_n, tile_n), tile_n)
        theirs = pl.ds(pl.multiple_of(landing(last) + i * tile_n, tile_n), tile_n)
        total = part[0, at].astype(f32) + recv[0, theirs].astype(f32) + r_sum[here].astype(f32)
        first[e, at] = layer_norm(
            residual_scale * tokens[at].astype(f32) + total, m_gain[...], m_shift[...]
        ).astype(bf16)

    to_mate.start()
    own_g[last].start()
    z_ends((DN,), 1)
    z_outward((DN,))
    z_mid((DN,), 2)
    for b in range(last, 0, -1):
        own_g[b].wait_recv()
        own_g[b - 1].start()
    wide_u = min(256, half)

    def up(q):
        @pl.loop(0, half // wide_u)
        def _(i):
            at = pl.ds(pl.multiple_of(i * wide_u, wide_u), wide_u)
            u = jnp.maximum(jnp.dot(first[q], up_g[:, at], preferred_element_type=f32), 0.0)
            hidden[q, :, at] = (u * u).astype(bf16)

    @at_inner
    def _():
        for h in range(hops):
            to_mate.parts[h].wait_recv()
            mate_g[last].parts[h].start()

    at_inner(lambda: relay_some(DN, 0, n_pc))
    own_g[0].wait_recv()
    partners_wait(UP)
    up(e)

    @at_end
    def _():
        for h in range(hops):
            to_mate.parts[h].wait_recv()
            mate_g[last].parts[h].start()

    at_end(lambda: relay_some(DN, 0, n_pc))
    for q in range(early):
        relay(DN, mate_k, q)
    for b in range(last, 0, -1):
        mate_g[b].wait_recv()
        mate_g[b - 1].start()
    for q in range(early, n_pc):
        relay(DN, mate_k, q)
    mate_g[0].wait_recv()
    up(1 - e)

    cw = 2 * rows // sub
    mine_h = pl.ds(pl.multiple_of(core * hs, hs), hs)
    away_h = pl.ds(pl.multiple_of((1 - core) * hs, hs), hs)
    chunks = []
    for of_k in order[2:3] + order[:2] + order[3:]:
        for i in range(sub):
            side = (p, 1 - p)[i] if sub == 2 else 0
            chunks.append((of_k, (2 * of_k + side) * rows, i))

    def cols_of(j):
        return pl.ds(pl.multiple_of(chunks[j][1], cw), cw)

    def s1(j):
        c = cols_of(j)
        return remote(
            part2.at[:, away_h, c],
            r_core.at[:, :, c],
            s1_send.at[j],
            s1_recv.at[j],
            {"tp": flip(1)},
        )

    def s2(j):
        c = cols_of(j)
        return remote(
            part2.at[1 - e, mine_h, c],
            r_mate.at[:, c],
            s2_send.at[j],
            s2_recv.at[j],
            {"fs": mate},
        )

    def s3(j, b):
        c = cols_of(j)
        return remote(
            part2.at[e, mine_h, c],
            r_x.at[b - 1, :, c],
            s3_send.at[b - 1, j],
            s3_recv.at[b - 1, j],
            {"tp": flip(1 << b)},
        )

    def product(j):
        c = cols_of(j)
        w = dn_g[c]

        @pl.loop(0, 2)
        def _(q):
            part2[q, :, c] = lax.dot_general(
                hidden[q], w, NT, preferred_element_type=f32
            ).astype(bf16)

        s1(j).start()

    def core_sum(j):
        c = cols_of(j)
        s1(j).wait_recv()
        part2[1 - e, mine_h, c] = (
            part2[1 - e, mine_h, c].astype(f32) + r_core[1 - e, :, c].astype(f32)
        ).astype(bf16)
        s2(j).start()

    def mate_sum(j):
        c = cols_of(j)
        s2(j).wait_recv()
        part2[e, mine_h, c] = (
            part2[e, mine_h, c].astype(f32)
            + r_core[e, :, c].astype(f32)
            + r_mate[:, c].astype(f32)
        ).astype(bf16)
        s3(j, 1).start()

    def x_sum(j, b):
        c = cols_of(j)
        s3(j, b - 1).wait()
        part2[e, mine_h, c] = (
            part2[e, mine_h, c].astype(f32) + r_x[b - 2, :, c].astype(f32)
        ).astype(bf16)
        s3(j, b).start()

    stages = [core_sum, mate_sum]
    for b in range(2, bits):
        stages.append(functools.partial(x_sum, b=b))
    n_ch = len(chunks)

    def later_sums(j):
        for i, stage in enumerate(stages[1:]):
            if 0 <= j - i < n_ch:
                stage(j - i)

    def chunk(j):
        if j % sub == sub - 1:
            for q in range(n_pc):
                f_wait(DN, 2 * chunks[j][0] + 1 - p, q)
        product(j)
        if j >= 1:
            core_sum(j - 1)

    summed = 0
    n_first = 3 * sub
    for j in range(n_first):
        chunk(j)
    for m in range(1, n_l // n_pc):
        ready = (m + 2) * sub - 1
        for q in range(n_pc):
            if summed < ready:
                later_sums(summed)
                summed += 1
            relay_some(DN, m * n_pc + q, m * n_pc + q + 1)
        for j in range((m + 2) * sub, (m + 3) * sub):
            chunk(j)
            if summed < j - 1:
                later_sums(summed)
                summed += 1
    core_sum(n_ch - 1)
    for j in range(summed, n_ch + len(stages) - 2):
        later_sums(j)

    n_out = o_send.shape[0]
    piece_rows = hs // n_out
    tile_o = min(piece_rows, 64)

    def out_rows(i):
        return pl.ds(pl.multiple_of(core * hs + i * piece_rows, piece_rows), piece_rows)

    def out_local(i):
        return pltpu.make_async_copy(
            result.at[pl.ds(i * piece_rows, piece_rows)], out.at[out_rows(i)], out_sem.at[i]
        )

    def out_remote(i):
        return remote(
            result.at[pl.ds(i * piece_rows, piece_rows)],
            out.at[out_rows(i)],
            o_send.at[i],
            o_recv.at[i],
            {"tp": flip(1)},
        )

    for j in range(n_ch):
        s3(j, last).wait_recv()
    for i in range(n_out):

        @pl.loop(0, piece_rows // tile_o)
        def _(ii):
            lo = i * piece_rows + ii * tile_o
            here = pl.ds(pl.multiple_of(lo, tile_o), tile_o)
            at = pl.ds(pl.multiple_of(core * hs + lo, tile_o), tile_o)
            total = part2[e, at].astype(f32) + r_x[last - 1, here].astype(f32)
            result[here] = layer_norm(
                residual_scale * first[e, at].astype(f32) + total, c_gain[...], c_shift[...]
            ).astype(bf16)

        out_local(i).start()
        out_remote(i).start()

    for a in range(6):
        f_drain(a)
    for c in [tok_z, sum_z, to_mate] + tok_g + reduces[0] + reduces[1] + own_g + mate_g:
        c.wait_send()
    for j in range(n_ch):
        s1(j).wait_send()
        s2(j).wait_send()
        s3(j, last).wait_send()
    for i in range(n_out):
        out_local(i).wait()
        out_remote(i).wait()


def local(
    tokens,
    gate_outer,
    gate_inner,
    conv_input,
    mixer_output,
    conv_taps,
    mixer_gain,
    mixer_shift,
    up_weight,
    down_weight,
    channel_gain,
    channel_shift,
):
    seq, width = tokens.shape
    rows, units = up_weight.shape
    chans = gate_outer.shape[1]
    half = units // 2
    n_fs = lax.axis_size("fs")
    n_tp = lax.axis_size("tp")
    bits = n_tp.bit_length() - 1
    nk = n_fs // 2
    hc = chans // 2
    sub = 2 if rows % 128 == 0 else 1
    n_ch = nk * sub
    hs = seq // 2
    n_out = 4
    n_pc = min(4, rows // 16)
    hops = 2
    n_t = bits + 1 + hops * (4 * bits + 2)
    mix = (gate_outer, gate_inner, conv_input, mixer_output)
    if hc % 128:
        mix = tuple(w.reshape(rows, 2, hc).swapaxes(0, 1) for w in mix)
        conv_taps = conv_taps.reshape(-1, 2, hc)
    vmem = pl.BlockSpec(memory_space=pltpu.VMEM)
    dma = pltpu.SemaphoreType.DMA
    return pl.pallas_call(
        functools.partial(kernel, n_fs, n_tp, sub, n_pc, hops),
        out_shape=jax.ShapeDtypeStruct((seq, width), bf16),
        in_specs=[vmem] * 12,
        out_specs=pl.BlockSpec(memory_space=pl.ANY),
        scratch_shapes=[
            pltpu.VMEM((4, width, hc), bf16),
            pltpu.VMEM((width, half), bf16),
            pltpu.VMEM((width, half), bf16),
            pltpu.VMEM((seq, width), bf16),
            pltpu.VMEM((2, seq, hc), f32),
            pltpu.VMEM((2, seq + 8, hc), f32),
            pltpu.VMEM((2, seq, hc), bf16),
            pltpu.VMEM((2, seq, width), bf16),
            pltpu.VMEM((2, seq, width), bf16),
            pltpu.VMEM((seq // n_tp, width), bf16),
            pltpu.VMEM((2, seq, width), bf16),
            pltpu.VMEM((2, seq, half), bf16),
            pltpu.VMEM((2, seq, width), bf16),
            pltpu.VMEM((2, hs, width), bf16),
            pltpu.VMEM((hs, width), bf16),
            pltpu.VMEM((bits - 1, hs, width), bf16),
            pltpu.VMEM((hs, width), bf16),
            dma((6, n_pc)),
            dma((n_out,)),
            dma((6, nk, n_pc)),
            dma((6, nk, n_pc)),
            dma((6, n_fs, n_pc)),
            dma((n_t,)),
            dma((n_t,)),
            dma((n_ch,)),
            dma((n_ch,)),
            dma((n_ch,)),
            dma((n_ch,)),
            dma((bits - 1, n_ch)),
            dma((bits - 1, n_ch)),
            dma((n_out,)),
            dma((n_out,)),
        ],
        compiler_params=pltpu.CompilerParams(
            collective_id=0, has_side_effects=True, vmem_limit_bytes=62 * 1024 * 1024
        ),
    )(
        tokens,
        *mix,
        conv_taps,
        mixer_gain.reshape(1, width),
        mixer_shift.reshape(1, width),
        up_weight,
        down_weight,
        channel_gain.reshape(1, width),
        channel_shift.reshape(1, width),
    )


def solution(mesh):
    in_specs = (
        P(("rep", "fs"), None),
        P("fs", "tp"),
        P("fs", "tp"),
        P("fs", "tp"),
        P("fs", "tp"),
        P(None, "tp"),
        P(),
        P(),
        P("fs", "tp"),
        P("fs", "tp"),
        P(),
        P(),
    )
    out_specs = P(("rep", "fs"), None)
    return jax.shard_map(local, mesh=mesh, in_specs=in_specs, out_specs=out_specs, check_vma=False)
```

time: 199 us -> 176 us (0.88)
  the two profiles are of different devices: /device:TPU:11 before, /device:TPU:0 now
where the time goes in v2:
time: 176 us
  Pallas kernels  173 us (98%)
  local copies, waits for them, and re-layouts  3.16 us (2%)
    pallas_call x1, Pallas kernels, local(): pl.pallas_call(functools.partial(kernel, n_fs, n_tp, sub, n_pc, hops), ou...  173 us

profile of v2, /device:TPU:0, one launch (start us, length us, event | category | flops | bytes accessed | tf_op | source)
XLA Modules:
  0.0 175.8 jit_solution(3848744539515335421)
XLA Ops:
  0.0 172.6 %shard_map.118 = bf16[512,2048]{1,0:T(8,128)(2,1)} custom-call(bf16[512,2048]{1,0:T(8,128)(2,1)} %tokens.1, bf16[256,256]{1,0:T(8,128)(2,1)} %w_go.1, bf16[256,256]{1,0:T(8,128)(2,1)} %w_gi.1, bf16[256,256]{1,0:T(8,128)(2,1)} %w_ci.1, bf16[256,256]{1,0:T(8,128)(2,1)} %w_mo.1, f32[3,256]{1,0:T(4,128)} %taps.1, f32[1,2048]{1,0:T(1,128)} %bitcast.4, ...), custom_call_target="tpu_custom_call" | custom-call | tf_op jit(solution)/shard_map/pallas_call | solution.py:729
  172.6 3.2 %copy.14 = bf16[512,2048]{1,0:T(8,128)(2,1)} copy(bf16[512,2048]{1,0:T(8,128)(2,1)} %shard_map.118) | data formatting | bytes 4194304

commit v3 on v2

--- a/solution.py
+++ b/solution.py
@@ -37,19 +37,25 @@
     sub,
     n_pc,
     hops,
-    tokens,
+    tokens_in,
     w_go,
     w_gi,
     w_ci,
     w_mo,
+    taps_in,
+    m_gain_in,
+    m_shift_in,
+    w_up,
+    w_dn,
+    c_gain_in,
+    c_shift_in,
+    out,
+    tokens,
     taps,
     m_gain,
     m_shift,
-    w_up,
-    w_dn,
     c_gain,
     c_shift,
-    out,
     mix_g,
     up_g,
     dn_g,
@@ -66,9 +72,9 @@
     r_core,
     r_mate,
     r_x,
-    result,
+    r_half,
     local_sem,
-    out_sem,
+    in_sem,
     z_sends,
     y_sends,
     f_recv,
@@ -80,6 +86,8 @@
     s2_recv,
     s3_send,
     s3_recv,
+    h_send,
+    h_recv,
     o_send,
     o_recv,
 ):
@@ -145,9 +153,16 @@
             copies.append(
                 pltpu.make_async_copy(source(a, e, q), held(a, f, q), local_sem.at[a, q])
             )
-    for c in copies:
-        c.start()
-
+    small = (
+        (tokens_in, tokens),
+        (taps_in, taps),
+        (m_gain_in, m_gain),
+        (m_shift_in, m_shift),
+        (c_gain_in, c_gain),
+        (c_shift_in, c_shift),
+    )
+    for i, (here, there) in enumerate(small):
+        copies.append(pltpu.make_async_copy(here, there, in_sem.at[i]))
     barrier = pltpu.get_barrier_semaphore()
     pl.semaphore_signal(barrier, inc=1, device_id={"fs": partner}, device_id_type=MESH)
     for i in range(1, nk):
@@ -156,6 +171,8 @@
         )
     for b in range(bits):
         pl.semaphore_signal(barrier, inc=1, device_id={"tp": flip(1 << b)}, device_id_type=MESH)
+    for c in copies:
+        c.start()
     pl.semaphore_wait(barrier, nk + bits)
 
     def z_copy(a, to_k, q):
@@ -320,7 +337,7 @@
     n_own = seq >> bits
     own_rows = span(starts[bits], n_own)
 
-    tok_z = t_copy(tokens.at[own_rows], tok_m.at[own_rows], {"fs": mate})
+    tok_z = t_copy(tokens_in.at[own_rows], tok_m.at[own_rows], {"fs": mate})
     tok_g = []
     for b in range(bits):
         ref = tok_m.at[span(starts[b + 1], seq >> (b + 1))]
@@ -576,6 +593,9 @@
         s1(j).start()
 
     def core_sum(j):
+        if j < n_half:
+            half_core(j)
+            return
         c = cols_of(j)
         s1(j).wait_recv()
         part2[1 - e, mine_h, c] = (
@@ -583,7 +603,105 @@
         ).astype(bf16)
         s2(j).start()
 
+    quarter = hs // 2
+    bit = (t // 2) % 2
+    own_q = shift(core * hs + bit * quarter, 0, quarter)
+    away_q = shift(core * hs + (1 - bit) * quarter, 0, quarter)
+    own_r = shift(bit * quarter, 0, quarter)
+    away_r = shift((1 - bit) * quarter, 0, quarter)
+
+    def h1(j):
+        c = cols_of(j)
+        return remote(
+            part2.at[1 - e, away_q, c],
+            r_half.at[:, c],
+            h_send.at[0, j],
+            h_recv.at[0, j],
+            {"tp": flip(2)},
+        )
+
+    def h2(j):
+        c = cols_of(j)
+        return remote(
+            part2.at[e, away_q, c],
+            r_x.at[0, away_r, c],
+            h_send.at[1, j],
+            h_recv.at[1, j],
+            {"tp": flip(2)},
+        )
+
+    def h2_wait(j):
+        c = cols_of(j)
+        remote(
+            part2.at[e, own_q, c],
+            r_x.at[0, own_r, c],
+            h_send.at[1, j],
+            h_recv.at[1, j],
+            {"tp": flip(2)},
+        ).wait_recv()
+
+    def h3(j):
+        c = cols_of(j)
+        return remote(
+            part2.at[1 - e, own_q, c],
+            r_mate.at[own_r, c],
+            s2_send.at[j],
+            s2_recv.at[j],
+            {"fs": mate},
+        )
+
+    def h4(j):
+        c = cols_of(j)
+        return remote(
+            part2.at[e, own_q, c],
+            r_x.at[0, own_r, c],
+            s3_send.at[0, j],
+            s3_recv.at[0, j],
+            {"tp": flip(2)},
+        )
+
+    def h4_wait(j):
+        c = cols_of(j)
+        remote(
+            part2.at[e, away_q, c],
+            r_x.at[0, away_r, c],
+            s3_send.at[0, j],
+            s3_recv.at[0, j],
+            {"tp": flip(2)},
+        ).wait_recv()
+
+    def plus(i, at, c, other):
+        part2[i, at, c] = (part2[i, at, c].astype(f32) + other.astype(f32)).astype(bf16)
+
+    def half_core(j):
+        c = cols_of(j)
+        s1(j).wait_recv()
+        plus(1 - e, away_q, c, r_core[1 - e, away_r, c])
+        h1(j).start()
+        plus(e, away_q, c, r_core[e, away_r, c])
+        plus(1 - e, own_q, c, r_core[1 - e, own_r, c])
+
+    def half_mid(j):
+        c = cols_of(j)
+        h1(j).wait_recv()
+        plus(1 - e, own_q, c, r_half[:, c])
+        h3(j).start()
+        h2(j).start()
+
+    def half_mate(j):
+        c = cols_of(j)
+        h3(j).wait_recv()
+        part2[e, own_q, c] = (
+            part2[e, own_q, c].astype(f32)
+            + r_core[e, own_r, c].astype(f32)
+            + r_mate[own_r, c].astype(f32)
+        ).astype(bf16)
+        h4(j).start()
+
     def mate_sum(j):
+        if j < n_half:
+            half_mate(j)
+            return
         c = cols_of(j)
         s2(j).wait_recv()
         part2[e, mine_h, c] = (
@@ -618,26 +736,54 @@
         product(j)
         if j >= 1:
             core_sum(j - 1)
-
-    summed = 0
+        if j < n_first and 0 <= j - 2 < n_half:
+            half_mid(j - 2)
+
+    n_half = 3 if bits == 2 else 0
+    summed = {at_inner: 0, at_end: 0}
+
+    def sums(where, n):
+        lo = summed[where]
+        stop = n_ch + len(stages) - 2
+        hi = min(stop, lo + n)
+        summed[where] = hi
+
+        @where
+        def _():
+            for j in range(lo, hi):
+                later_sums(j)
+
     n_first = 3 * sub
+    mids = n_pc if nk > 2 else 0
+
+    def ahead(where, q):
+        if 0 <= q < mids:
+            where(lambda: relay_some(DN, n_pc + q, n_pc + q + 1))
+
     for j in range(n_first):
         chunk(j)
+        ahead(at_inner, j - 0)
+        ahead(at_end, j - 3)
+        if j >= 3:
+            sums(at_end, 1)
+    for j in range(max(0, n_first - 2), n_half):
+        half_mid(j)
     for m in range(1, n_l // n_pc):
-        ready = (m + 2) * sub - 1
         for q in range(n_pc):
-            if summed < ready:
-                later_sums(summed)
-                summed += 1
-            relay_some(DN, m * n_pc + q, m * n_pc + q + 1)
+            if m > 1:
+                relay_some(DN, m * n_pc + q, m * n_pc + q + 1)
+            else:
+                ahead(at_inner, n_first + q - 0)
+                ahead(at_end, n_first + q - 3)
+            if q < 4:
+                sums(at_inner, 1)
+            if q < 2:
+                sums(at_end, 1)
         for j in range((m + 2) * sub, (m + 3) * sub):
             chunk(j)
-            if summed < j - 1:
-                later_sums(summed)
-                summed += 1
     core_sum(n_ch - 1)
-    for j in range(summed, n_ch + len(stages) - 2):
-        later_sums(j)
+    sums(at_inner, n_ch)
+    sums(at_end, n_ch)
 
     n_out = o_send.shape[0]
     piece_rows = hs // n_out
@@ -646,14 +792,9 @@
     def out_rows(i):
         return pl.ds(pl.multiple_of(core * hs + i * piece_rows, piece_rows), piece_rows)
 
-    def out_local(i):
-        return pltpu.make_async_copy(
-            result.at[pl.ds(i * piece_rows, piece_rows)], out.at[out_rows(i)], out_sem.at[i]
-        )
-
     def out_remote(i):
         return remote(
-            result.at[pl.ds(i * piece_rows, piece_rows)],
+            out.at[out_rows(i)],
             out.at[out_rows(i)],
             o_send.at[i],
             o_recv.at[i],
@@ -661,7 +802,11 @@
         )
 
     for j in range(n_ch):
-        s3(j, last).wait_recv()
+        if j < n_half:
+            h2_wait(j)
+            h4_wait(j)
+        else:
+            s3(j, last).wait_recv()
     for i in range(n_out):
 
         @pl.loop(0, piece_rows // tile_o)
@@ -670,11 +815,10 @@
             here = pl.ds(pl.multiple_of(lo, tile_o), tile_o)
             at = pl.ds(pl.multiple_of(core * hs + lo, tile_o), tile_o)
             total = part2[e, at].astype(f32) + r_x[last - 1, here].astype(f32)
-            result[here] = layer_norm(
+            out[at] = layer_norm(
                 residual_scale * first[e, at].astype(f32) + total, c_gain[...], c_shift[...]
             ).astype(bf16)
 
-        out_local(i).start()
         out_remote(i).start()
 
     for a in range(6):
@@ -683,10 +827,13 @@
         c.wait_send()
     for j in range(n_ch):
         s1(j).wait_send()
-        s2(j).wait_send()
-        s3(j, last).wait_send()
+        if j < n_half:
+            for c in (h1(j), h2(j), h3(j), h4(j)):
+                c.wait_send()
+        else:
+            s2(j).wait_send()
+            s3(j, last).wait_send()
     for i in range(n_out):
-        out_local(i).wait()
         out_remote(i).wait()
 
 
@@ -719,19 +866,25 @@
     n_out = 4
     n_pc = min(4, rows // 16)
     hops = 2
+    vmem_bytes = 67043328 - 65536
     n_t = bits + 1 + hops * (4 * bits + 2)
     mix = (gate_outer, gate_inner, conv_input, mixer_output)
     if hc % 128:
         mix = tuple(w.reshape(rows, 2, hc).swapaxes(0, 1) for w in mix)
         conv_taps = conv_taps.reshape(-1, 2, hc)
-    vmem = pl.BlockSpec(memory_space=pltpu.VMEM)
     dma = pltpu.SemaphoreType.DMA
     return pl.pallas_call(
         functools.partial(kernel, n_fs, n_tp, sub, n_pc, hops),
-        out_shape=jax.ShapeDtypeStruct((seq, width), bf16),
-        in_specs=[vmem] * 12,
-        out_specs=pl.BlockSpec(memory_space=pl.ANY),
+        out_shape=pltpu.VMEM((seq, width), bf16),
+        in_specs=[pl.BlockSpec(memory_space=pl.ANY)] * 12,
+        out_specs=pl.BlockSpec(memory_space=pltpu.VMEM),
         scratch_shapes=[
+            pltpu.VMEM((seq, width), bf16),
+            pltpu.VMEM(conv_taps.shape, f32),
+            pltpu.VMEM((1, width), f32),
+            pltpu.VMEM((1, width), f32),
+            pltpu.VMEM((1, width), f32),
+            pltpu.VMEM((1, width), f32),
             pltpu.VMEM((4, width, hc), bf16),
             pltpu.VMEM((width, half), bf16),
             pltpu.VMEM((width, half), bf16),
@@ -748,9 +901,9 @@
             pltpu.VMEM((2, hs, width), bf16),
             pltpu.VMEM((hs, width), bf16),
             pltpu.VMEM((bits - 1, hs, width), bf16),
-            pltpu.VMEM((hs, width), bf16),
+            pltpu.VMEM((hs // 2, width), bf16),
             dma((6, n_pc)),
-            dma((n_out,)),
+            dma((6,)),
             dma((6, nk, n_pc)),
             dma((6, nk, n_pc)),
             dma((6, n_fs, n_pc)),
@@ -762,11 +915,13 @@
             dma((n_ch,)),
             dma((bits - 1, n_ch)),
             dma((bits - 1, n_ch)),
+            dma((2, n_ch)),
+            dma((2, n_ch)),
             dma((n_out,)),
             dma((n_out,)),
         ],
         compiler_params=pltpu.CompilerParams(
-            collective_id=0, has_side_effects=True, vmem_limit_bytes=62 * 1024 * 1024
+            collective_id=0, has_side_effects=True, vmem_limit_bytes=vmem_bytes - 2 * seq * width
         ),
     )(
         tokens,

time: 176 us -> 168 us (0.955)
  the two profiles are of different devices: /device:TPU:0 before, /device:TPU:11 now
where the time goes in v3:
time: 168 us; the launch traced here: 167 us
  Pallas kernels  165 us (98%)
    pallas_call x1, Pallas kernels, local(): pl.pallas_call(functools.partial(kernel, n_fs, n_tp, sub, n_pc, hops), ou...  165 us

profile of v3, /device:TPU:11, one launch (start us, length us, event | category | flops | bytes accessed | tf_op | source)
XLA Modules:
  0.0 166.8 jit_solution(4654064240373763024)
XLA Ops:
  0.0 165.5 %shard_map.118 = bf16[512,2048]{1,0:T(8,128)(2,1)S(1)} custom-call(bf16[512,2048]{1,0:T(8,128)(2,1)} %tokens_in.1, bf16[256,256]{1,0:T(8,128)(2,1)} %w_go.1, bf16[256,256]{1,0:T(8,128)(2,1)} %w_gi.1, bf16[256,256]{1,0:T(8,128)(2,1)} %w_ci.1, bf16[256,256]{1,0:T(8,128)(2,1)} %w_mo.1, f32[3,256]{1,0:T(4,128)} %taps_in.1, f32[1,2048]{1,0:T(1,128)} %bitcast.4, ...), custom_call_target="tpu_custom_call" | custom-call | tf_op jit(solution)/shard_map/pallas_call | solution.py:876
  165.5 1.3 copy.14

commit v4 on v3

--- a/solution.py
+++ b/solution.py
@@ -394,10 +394,6 @@
     for a in ins:
         partners_wait(a)
 
-    @at_inner
-    def _():
-        relay_all(UP, mate_k)
-
     at_end(lambda: y_own(DN))
 
     pad = zpad.shape[1] - seq
@@ -468,6 +464,11 @@
     @at_end
     def _():
         relay_all(UP, mate_k)
+
+    @at_inner
+    def _():
+        for q in range(0, n_pc):
+            relay(UP, mate_k, q)
 
     at_inner(lambda: relay_some(UP, 0, n_pc))
     for h in range(hops):
@@ -496,11 +497,11 @@
     to_mate.start()
     own_g[last].start()
     z_ends((DN,), 1)
-    z_outward((DN,))
     z_mid((DN,), 2)
     for b in range(last, 0, -1):
         own_g[b].wait_recv()
         own_g[b - 1].start()
+    z_outward((DN,))
     wide_u = min(256, half)
 
     def up(q):
@@ -763,7 +764,7 @@
     for j in range(n_first):
         chunk(j)
         ahead(at_inner, j - 0)
-        ahead(at_end, j - 3)
+        ahead(at_end, j - 2)
         if j >= 3:
             sums(at_end, 1)
     for j in range(max(0, n_first - 2), n_half):
@@ -774,7 +775,7 @@
                 relay_some(DN, m * n_pc + q, m * n_pc + q + 1)
             else:
                 ahead(at_inner, n_first + q - 0)
-                ahead(at_end, n_first + q - 3)
+                ahead(at_end, n_first + q - 2)
             if q < 4:
                 sums(at_inner, 1)
             if q < 2:

time: 168 us -> 162 us (0.964)
  Pallas kernels: 165 us -> 161 us
    pallas_call x1, Pallas kernels: 165 us -> 161 us  [local(): pl.pallas_call(functools.partial(kernel, n_fs, n_tp, sub, n_pc, hops), ou...]
where the time goes in v4:
time: 162 us
  Pallas kernels  161 us (99%)
    pallas_call x1, Pallas kernels, local(): pl.pallas_call(functools.partial(kernel, n_fs, n_tp, sub, n_pc, hops), ou...  161 us

profile of v4, /device:TPU:11, one launch (start us, length us, event | category | flops | bytes accessed | tf_op | source)
XLA Modules:
  0.0 161.9 jit_solution(15585879972999497598)
XLA Ops:
  0.0 160.6 %shard_map.118 = bf16[512,2048]{1,0:T(8,128)(2,1)S(1)} custom-call(bf16[512,2048]{1,0:T(8,128)(2,1)} %tokens_in.1, bf16[256,256]{1,0:T(8,128)(2,1)} %w_go.1, bf16[256,256]{1,0:T(8,128)(2,1)} %w_gi.1, bf16[256,256]{1,0:T(8,128)(2,1)} %w_ci.1, bf16[256,256]{1,0:T(8,128)(2,1)} %w_mo.1, f32[3,256]{1,0:T(4,128)} %taps_in.1, f32[1,2048]{1,0:T(1,128)} %bitcast.4, ...), custom_call_target="tpu_custom_call" | custom-call | tf_op jit(solution)/shard_map/pallas_call | solution.py:877
  160.6 1.3 copy.14

commit v5 on v4

--- a/solution.py
+++ b/solution.py
@@ -865,7 +865,7 @@
     n_ch = nk * sub
     hs = seq // 2
     n_out = 4
-    n_pc = min(4, rows // 16)
+    n_pc = min(2, rows // 16)
     hops = 2
     vmem_bytes = 67043328 - 65536
     n_t = bits + 1 + hops * (4 * bits + 2)

time: 162 us -> 161 us (level)
  no operation moved by 1% of the time
where the time goes in v5:
time: 161 us
  Pallas kernels  160 us (99%)
    pallas_call x1, Pallas kernels, local(): pl.pallas_call(functools.partial(kernel, n_fs, n_tp, sub, n_pc, hops), ou...  160 us

profile of v5, /device:TPU:11, one launch (start us, length us, event | category | flops | bytes accessed | tf_op | source)
XLA Modules:
  0.0 161.2 jit_solution(13513786386566129993)
XLA Ops:
  0.0 159.9 %shard_map.118 = bf16[512,2048]{1,0:T(8,128)(2,1)S(1)} custom-call(bf16[512,2048]{1,0:T(8,128)(2,1)} %tokens_in.1, bf16[256,256]{1,0:T(8,128)(2,1)} %w_go.1, bf16[256,256]{1,0:T(8,128)(2,1)} %w_gi.1, bf16[256,256]{1,0:T(8,128)(2,1)} %w_ci.1, bf16[256,256]{1,0:T(8,128)(2,1)} %w_mo.1, f32[3,256]{1,0:T(4,128)} %taps_in.1, f32[1,2048]{1,0:T(1,128)} %bitcast.4, ...), custom_call_target="tpu_custom_call" | custom-call | tf_op jit(solution)/shard_map/pallas_call | solution.py:877
  159.9 1.3 copy.14
